TPU v7x, 32 devices: a whole 2x2x4 slice. The times are simulated.
32 devices in a mesh: ep: 8 (over z, x), tp: 4 (over y, core).
Axes of the slice: x: 2, y: 2, z: 4, core: 2. Of those that a mesh axis runs over, the one named last changes fastest.
Arguments:
- tokens: bfloat16 [192, 4096], P('ep'), may hold values from -6 to 6
- delta_state: float32 [192, 16, 128, 128], P('ep', 'tp'), may hold values from -0.625 to 0.625
- attn_gain: float32 [4096], replicated, may hold values from 0.1 to 1.9
- query_weight: bfloat16 [4096, 2048], P('ep', 'tp'), may hold values from -0.09375 to 0.09375
- key_weight: bfloat16 [4096, 2048], P('ep', 'tp'), may hold values from -0.09375 to 0.09375
- value_weight: bfloat16 [4096, 2048], P('ep', 'tp'), may hold values from -0.09375 to 0.09375
- decay_weight: bfloat16 [4096, 16], replicated, may hold values from -0.09375 to 0.09375
- beta_weight: bfloat16 [4096, 16], replicated, may hold values from -0.09375 to 0.09375
- decay_rate: float32 [16], P('tp'), may hold values from 0.05 to 3
- head_gain: float32 [128], replicated, may hold values from 0.1 to 1.9
- output_weight: bfloat16 [2048, 4096], P('tp'), may hold values from -0.125 to 0.125
- ffn_gain: float32 [4096], replicated, may hold values from 0.1 to 1.9
- expert_ids: int32 [192, 2], P('ep'), may hold values from 0 to 7, all different within a row; in each aligned block of 24 rows (0 to 23, 24 to 47, ...) at most 12 rows name the same one
- group_prob: float32 [192], P('ep'), may hold values from 0.3 to 1
- expert_logit: float32 [192, 2], P('ep'), may hold values from -8 to 8
- expert_gate: bfloat16 [8, 4096, 1024], P('ep', None, 'tp'), may hold values from -0.09375 to 0.09375
- expert_up: bfloat16 [8, 4096, 1024], P('ep', None, 'tp'), may hold values from -0.09375 to 0.09375
- expert_down: bfloat16 [8, 1024, 4096], P('ep', 'tp'), may hold values from -0.1875 to 0.1875
- dense_gate: bfloat16 [4096, 4096], P('tp', 'ep'), may hold values from -0.09375 to 0.09375
- dense_up: bfloat16 [4096, 4096], P('tp', 'ep'), may hold values from -0.09375 to 0.09375
- dense_down: bfloat16 [4096, 4096], P('ep', 'tp'), may hold values from -0.09375 to 0.09375
- dense_mix: float32 [4096], P('tp'), may hold values from -3 to 3
Outputs:
- mixed_out: bfloat16 [192, 4096], P('ep', 'tp')
- new_state: float32 [192, 16, 128, 128], P('ep', 'tp')
Inputs may be any that keep to these rules, and one draw needn't show every extreme that they name: `expert_ids`: each row names 2 different experts. Among the rows of one device (aligned blocks of 24 rows) no expert is named by more than 12 rows, and in every draw some expert reaches 12 in some block.
All inputs are finite; a program needn't handle non-finite values.
Results may differ from a plain program's by a relative error of at most 0.02.
Values may be sent and summed in bfloat16 or wider, within the bound.
A program may use at most 64 MiB of HBM per device.

v0:
```python
import jax
import jax.numpy as jnp
from jax import lax
from jax.sharding import PartitionSpec as P

EPS = 1e-06


def rms_scale(values, gain):
    mean_sq = jnp.mean(values * values, axis=-1, keepdims=True)
    return values * lax.rsqrt(mean_sq + EPS) * gain


def unit_rows(values):
    return values * lax.rsqrt(jnp.sum(values * values, axis=-1, keepdims=True) + EPS)


def per_device(
    tokens,
    delta_state,
    attn_gain,
    query_weight,
    key_weight,
    value_weight,
    decay_weight,
    beta_weight,
    decay_rate,
    head_gain,
    output_weight,
    ffn_gain,
    expert_ids,
    group_prob,
    expert_logit,
    expert_gate,
    expert_up,
    expert_down,
    dense_gate,
    dense_up,
    dense_down,
    dense_mix,
):
    seq_rows = tokens.shape[0]
    head_count = delta_state.shape[1]
    head_size = delta_state.shape[2]
    width_local = head_count * head_size
    tp_index = lax.axis_index("tp")
    residual = tokens.astype(jnp.float32)
    normed = rms_scale(residual, attn_gain).astype(jnp.bfloat16)
    spread = lax.all_to_all(normed, "ep", split_axis=1, concat_axis=0, tiled=True)
    joined = jnp.concatenate((query_weight, key_weight, value_weight), axis=1)
    summed = lax.psum_scatter(
        jnp.dot(spread, joined, preferred_element_type=jnp.float32).astype(jnp.bfloat16),
        "ep",
        scatter_dimension=0,
        tiled=True,
    ).astype(jnp.float32)
    query_sum = summed[:, :width_local]
    key_sum = summed[:, width_local : 2 * width_local]
    value_sum = summed[:, 2 * width_local :]

    def heads_of(values):
        rounded = lax.optimization_barrier(values.astype(jnp.bfloat16))
        return rounded.astype(jnp.float32).reshape(seq_rows, head_count, head_size)

    query_unit = unit_rows(heads_of(query_sum)) * head_size ** (-0.5)
    key_unit = unit_rows(heads_of(key_sum))
    value_heads = heads_of(value_sum)
    decay_cols = lax.dynamic_slice_in_dim(decay_weight, tp_index * head_count, head_count, 1)
    beta_cols = lax.dynamic_slice_in_dim(beta_weight, tp_index * head_count, head_count, 1)
    decay_pre = jnp.dot(normed, decay_cols, preferred_element_type=jnp.float32)
    decay = jnp.exp(-decay_rate * jax.nn.softplus(decay_pre))
    beta_gate = jax.nn.sigmoid(jnp.dot(normed, beta_cols, preferred_element_type=jnp.float32))
    recalled = jnp.einsum("bhk,bhkv->bhv", key_unit, delta_state, precision=lax.Precision.HIGHEST)
    correction = beta_gate[..., None] * (value_heads - decay[..., None] * recalled)
    new_state = (
        decay[..., None, None] * delta_state + key_unit[..., :, None] * correction[..., None, :]
    )
    read_out = jnp.einsum("bhk,bhkv->bhv", query_unit, new_state, precision=lax.Precision.HIGHEST)
    head_out = rms_scale(read_out, head_gain).astype(jnp.bfloat16).reshape(seq_rows, width_local)
    attn_part = jnp.dot(head_out, output_weight, preferred_element_type=jnp.float32)
    attn_sum = lax.psum(attn_part.astype(jnp.bfloat16), "tp").astype(jnp.float32)
    middle = residual + attn_sum
    ffn_in = rms_scale(middle, ffn_gain).astype(jnp.bfloat16)
    slice_width = dense_gate.shape[0]
    hidden_width = dense_gate.shape[1]
    own_columns = lax.dynamic_slice_in_dim(ffn_in, tp_index * slice_width, slice_width, 1)
    gate_up = jnp.concatenate((dense_gate, dense_up), axis=1)
    dense_part = jnp.dot(
        lax.all_gather(own_columns, "ep", axis=0, tiled=True),
        gate_up,
        preferred_element_type=jnp.float32,
    )
    dense_sum = lax.psum(dense_part.astype(jnp.bfloat16), "tp").astype(jnp.float32)
    dense_hidden = (jax.nn.silu(dense_sum[:, :hidden_width]) * dense_sum[:, hidden_width:]).astype(
        jnp.bfloat16
    )
    dense_out = lax.psum_scatter(
        jnp.dot(dense_hidden, dense_down, preferred_element_type=jnp.float32).astype(jnp.bfloat16),
        "ep",
        scatter_dimension=0,
        tiled=True,
    ).astype(jnp.float32)
    expert_count = lax.axis_size("ep")
    top_count = expert_ids.shape[1]
    capacity = max(2, 2 * seq_rows * top_count // expert_count)
    pair_ids = expert_ids.reshape(-1)
    onehot = (pair_ids[:, None] == jnp.arange(expert_count, dtype=jnp.int32)[None, :]).astype(
        jnp.int32
    )
    ranks = jnp.sum(onehot * (jnp.cumsum(onehot, axis=0) - 1), axis=1)
    places = pair_ids * capacity + ranks
    dispatch = (
        jnp.arange(expert_count * capacity, dtype=jnp.int32)[:, None] == places[None, :]
    ).astype(jnp.bfloat16)
    repeated = jnp.repeat(ffn_in, top_count, axis=0)
    outgoing = jnp.dot(dispatch, repeated, preferred_element_type=jnp.float32).astype(jnp.bfloat16)
    outgoing = outgoing.reshape(expert_count, capacity, ffn_in.shape[1])
    arrived = lax.all_to_all(outgoing, "ep", split_axis=0, concat_axis=0, tiled=True)
    gate_vals = jnp.einsum(
        "snd,df->snf", arrived, expert_gate[0], preferred_element_type=jnp.float32
    )
    up_vals = jnp.einsum("snd,df->snf", arrived, expert_up[0], preferred_element_type=jnp.float32)
    expert_hidden = (jax.nn.silu(gate_vals) * up_vals).astype(jnp.bfloat16)
    partial_value = jnp.einsum(
        "snf,fd->snd", expert_hidden, expert_down[0], preferred_element_type=jnp.float32
    )
    summed_cols = lax.psum_scatter(
        partial_value.astype(jnp.bfloat16), "tp", scatter_dimension=2, tiled=True
    )
    returned = lax.all_to_all(summed_cols, "ep", split_axis=0, concat_axis=0, tiled=True)
    flat_back = returned.reshape(expert_count * capacity, slice_width)
    picked = (
        jnp.take(flat_back, places, axis=0)
        .astype(jnp.float32)
        .reshape(seq_rows, top_count, slice_width)
    )
    logit_exp = jnp.exp(expert_logit)
    route_weight = group_prob[:, None] * logit_exp / jnp.sum(logit_exp, axis=1, keepdims=True)
    expert_mix = jnp.sum(route_weight[..., None] * picked, axis=1)
    own_middle = lax.dynamic_slice_in_dim(middle, tp_index * slice_width, slice_width, 1)
    mixed_out = (own_middle + jax.nn.sigmoid(dense_mix) * dense_out + expert_mix).astype(
        jnp.bfloat16
    )
    return (mixed_out, new_state)


def solution(mesh):
    return jax.shard_map(
        per_device,
        mesh=mesh,
        in_specs=(
            P("ep", None),
            P("ep", "tp", None, None),
            P(),
            P("ep", "tp"),
            P("ep", "tp"),
            P("ep", "tp"),
            P(),
            P(),
            P("tp"),
            P(),
            P("tp", None),
            P(),
            P("ep", None),
            P("ep"),
            P("ep", None),
            P("ep", None, "tp"),
            P("ep", None, "tp"),
            P("ep", "tp", None),
            P("tp", "ep"),
            P("tp", "ep"),
            P("ep", "tp"),
            P("tp"),
        ),
        out_specs=(P("ep", "tp"), P("ep", "tp", None, None)),
        check_vma=False,
    )
```

profile of v0, /device:TPU:0, one launch (start us, length us, event | category | flops | bytes accessed | tf_op | source)
XLA Modules:
  0.0 333.8 jit_solution(11705922929324244987)
XLA Ops:
  7.2 1.2 fusion.28
  9.6 15.0 %all_to_all.29 = bf16[24,8,512]{2,0,1:T(8,128)(2,1)S(1)} all-to-all(bf16[24,8,512]{2,0,1:T(8,128)(2,1)S(1)} %bitcast.59), channel_id=1, replica_groups=mesh['ep'=8,'tp'=4] {'ep'}, dimensions={1} | all-to-all | bytes 393216 | tf_op jit(solution)/shard_map/all_to_all | solution.py:49
  24.6 2.7 convolution_convert_fusion.3
  30.1 58.6 %reduce-scatter.4.cloned.1.call-done = bf16[24,1536]{1,0:T(8,128)(2,1)} async-done(((bf16[192,1536]{1,0:T(8,128)(2,1)}), bf16[24,1536]{1,0:T(8,128)(2,1)}) %reduce-scatter.4.cloned.1.call-update) | async-done | bytes 73744 | tf_op jit(solution)/shard_map/reduce_scatter | solution.py:51
  89.8 8.1 %fusion.59 = f32[24,4,1,128]{3,2,1,0:T(1,128)S(1)} fusion(f32[24,4,128,1]{2,3,1,0:T(1,128)S(1)} %bitcast.60, f32[24,4,128,128]{3,2,1,0:T(8,128)} %param.23), kind=kOutput, calls=%fused_computation.93 | convolution fusion | flops 18874368 | bytes 6389760 | tf_op jit(solution)/shard_map/bhk,bhkv->bhv/dot_general | solution.py:73
  98.1 3.9 %multiply_add_fusion = f32[24,4,128,128]{3,2,1,0:T(8,128)} fusion(f32[24,4,128,128]{3,2,1,0:T(8,128)S(1)} %copy-done.1, f32[24,4,128]{2,1,0:T(4,128)S(1)} %subtract_multiply_fusion, f32[24,4,128]{2,1,0:T(4,128)S(1)} %broadcast_multiply_fusion, f32[24,4]{1,0:T(8,128)S(1)} %copy.67), kind=kLoop, calls=%fused_computation.1 | loop fusion | flops 4718592 | bytes 12681600 | tf_op jit(solution)/shard_map/add | solution.py:76
  102.2 7.5 %fusion.60 = f32[24,4,1,128]{3,2,1,0:T(1,128)S(1)} fusion(f32[24,4,128,1]{2,3,1,0:T(1,128)S(1)} %bitcast.63, f32[24,4,128,128]{3,2,1,0:T(8,128)} %multiply_add_fusion), kind=kOutput, calls=%fused_computation.94 | convolution fusion | flops 18874368 | bytes 6389760 | tf_op jit(solution)/shard_map/bhk,bhkv->bhv/dot_general | solution.py:78
  109.9 1.4 convolution_convert_fusion.2
  111.3 31.2 %all-reduce.3.cloned.1.call-done = bf16[24,4096]{1,0:T(8,128)(2,1)} async-done(((bf16[24,4096]{1,0:T(8,128)(2,1)}), bf16[24,4096]{1,0:T(8,128)(2,1)}) %all-reduce.3.cloned.1.call-update) | async-done | bytes 196624 | tf_op jit(solution)/shard_map/psum | solution.py:81
  142.5 1.8 convert_add_fusion
  146.2 1.2 reshape.153
  147.4 5.5 %all-to-all-start.1 = ((bf16[8,12,4096]{2,1,0:T(8,128)(2,1)}), bf16[8,12,4096]{2,1,0:T(8,128)(2,1)S(1)}, u32[]{:S(2)}, u32[]{:S(2)}) async-start(bf16[8,12,4096]{2,1,0:T(8,128)(2,1)} %reshape.153), calls=%async_computation.3 | async-start | bytes 2097152 | tf_op jit(solution)/shard_map/all_to_all | solution.py:118
  153.0 45.7 %all_gather.3 = bf16[192,1024]{1,0:T(8,128)(2,1)S(1)} all-gather(bf16[24,1024]{1,0:T(8,128)(2,1)S(1)} %constant_dynamic-slice_fusion), channel_id=1, replica_groups=mesh['ep'=8,'tp'=4] {'ep'}, dimensions={0}, use_global_device_ids=true | all-gather | bytes 442368 | tf_op jit(solution)/shard_map/all_gather | solution.py:89
  198.6 2.9 fusion.14
  201.6 2.0 fusion.7
  203.7 3.9 %convolution_convert_fusion = bf16[8,12,4096]{2,1,0:T(8,128)(2,1)} fusion(bf16[1,256,4096]{2,1,0:T(8,128)(2,1)S(1)} %copy-done, bf16[8,12,4096]{2,1,0:T(8,128)(2,1)S(1)} %all-to-all-done.1, bf16[1,4096,256]{2,1,0:T(8,128)(2,1)} %param.38, f32[8,12,256]{2,1,0:T(8,128)S(1)} %fusion.7), kind=kOutput, calls=%fused_computation.2 | convolution fusion | flops 403193856 | bytes 5865472 | tf_op jit(solution)/shard_map/snf,fd->snd/dot_general | solution.py:124
  207.9 25.3 %all-reduce.5.cloned.1.call-done = bf16[192,1024]{1,0:T(8,128)(2,1)} async-done(((bf16[192,1024]{1,0:T(8,128)(2,1)}), bf16[192,1024]{1,0:T(8,128)(2,1)}) %all-reduce.5.cloned.1.call-update) | async-done | bytes 393232 | tf_op jit(solution)/shard_map/psum | solution.py:93
  233.2 1.1 convert_element_type.71
  234.3 2.4 convolution_convert_fusion.4
  236.9 23.5 %reduce-scatter.8.cloned.1.call-done = bf16[8,12,1024]{2,1,0:T(8,128)(2,1)} async-done(((bf16[8,12,4096]{2,1,0:T(8,128)(2,1)}), bf16[8,12,1024]{2,1,0:T(8,128)(2,1)}) %reduce-scatter.8.cloned.1.call-update) | async-done | bytes 196624 | tf_op jit(solution)/shard_map/reduce_scatter | solution.py:127
  260.4 5.5 %all-to-all-start.2 = ((bf16[8,12,1024]{2,1,0:T(8,128)(2,1)}), bf16[8,12,1024]{2,1,0:T(8,128)(2,1)S(1)}, u32[]{:S(2)}, u32[]{:S(2)}) async-start(bf16[8,12,1024]{2,1,0:T(8,128)(2,1)} %reduce-scatter.8.cloned.1.call-done), calls=%async_computation.5 | async-start | bytes 524288 | tf_op jit(solution)/shard_map/all_to_all | solution.py:130
  266.1 9.1 %all-to-all-done.2 = bf16[8,12,1024]{2,1,0:T(8,128)(2,1)S(1)} async-done(((bf16[8,12,1024]{2,1,0:T(8,128)(2,1)}), bf16[8,12,1024]{2,1,0:T(8,128)(2,1)S(1)}, u32[]{:S(2)}, u32[]{:S(2)}) %all-to-all-start.2) | async-done | bytes 196640 | tf_op jit(solution)/shard_map/all_to_all | solution.py:130
  276.4 49.3 %reduce-scatter.6.cloned.1.call-done = bf16[24,1024]{1,0:T(8,128)(2,1)} async-done(((bf16[192,1024]{1,0:T(8,128)(2,1)}), bf16[24,1024]{1,0:T(8,128)(2,1)}) %reduce-scatter.6.cloned.1.call-update) | async-done | bytes 49168 | tf_op jit(solution)/shard_map/reduce_scatter | solution.py:97
  325.7 1.6 add_convert_fusion
  (84 shorter events, 9.4 us)
Async XLA Ops:
  7.2 196.5 %copy-start = (bf16[1,256,4096]{2,1,0:T(8,128)(2,1)S(1)}, bf16[1,256,4096]{2,1,0:T(8,128)(2,1)}, u32[]{:S(2)}) copy-start(bf16[1,256,4096]{2,1,0:T(8,128)(2,1)} %param.39) | copy-start | bytes 6291460
  7.2 81.6 %reduce-scatter.4.cloned.1.call-start = ((), (), s32[]{:S(2)}) async-start(), calls=%async_computation.6 | async-start | bytes 663552 | tf_op jit(solution)/shard_map/reduce_scatter | solution.py:51
  9.5 17.8 %copy-start.10 = (f32[4]{0:T(128)S(1)}, f32[4]{0:T(128)}, u32[]{:S(2)}) copy-start(f32[4]{0:T(128)} %param.30) | copy-start | bytes 52
  9.5 20.1 %copy-start.5 = (s32[24,2]{0,1:T(2,128)S(1)}, s32[24,2]{0,1:T(2,128)}, u32[]{:S(2)}) copy-start(s32[24,2]{0,1:T(2,128)} %param.34) | copy-start | bytes 580
  27.3 115.2 %all-reduce.3.cloned.1.call-start = ((), (), s32[]{:S(2)}) async-start(), calls=%async_computation.7 | async-start | bytes 393216 | tf_op jit(solution)/shard_map/psum | solution.py:81
  89.8 8.2 %copy-start.1 = (f32[24,4,128,128]{3,2,1,0:T(8,128)S(1)}, f32[24,4,128,128]{3,2,1,0:T(8,128)}, u32[]{:S(2)}) copy-start(f32[24,4,128,128]{3,2,1,0:T(8,128)} %param.23) | copy-start | bytes 18874372
  102.2 7.6 %copy-start.8 = (f32[128]{0:T(128)S(1)}, f32[128]{0:T(128)}, u32[]{:S(2)}) copy-start(f32[128]{0:T(128)} %param.31) | copy-start | bytes 1540
  102.2 7.7 %copy-start.2 = (bf16[512,4096]{1,0:T(8,128)(2,1)S(1)}, bf16[512,4096]{1,0:T(8,128)(2,1)}, u32[]{:S(2)}) copy-start(bf16[512,4096]{1,0:T(8,128)(2,1)} %param.32) | copy-start | bytes 12582916
  109.7 32.8 %copy-start.3 = (bf16[24,4096]{1,0:T(8,128)(2,1)S(1)}, bf16[24,4096]{1,0:T(8,128)(2,1)}, u32[]{:S(2)}) copy-start(bf16[24,4096]{1,0:T(8,128)(2,1)} %param.22) | copy-start | bytes 589828
  109.7 34.7 %copy-start.4 = (f32[4096]{0:T(1024)S(1)}, f32[4096]{0:T(1024)}, u32[]{:S(2)}) copy-start(f32[4096]{0:T(1024)} %param.33) | copy-start | bytes 49156
  147.4 54.2 %all-to-all-start.1 = ((bf16[8,12,4096]{2,1,0:T(8,128)(2,1)}), bf16[8,12,4096]{2,1,0:T(8,128)(2,1)S(1)}, u32[]{:S(2)}, u32[]{:S(2)}) async-start(bf16[8,12,4096]{2,1,0:T(8,128)(2,1)} %reshape.153), calls=%async_computation.3 | async-start | bytes 2097152 | tf_op jit(solution)/shard_map/all_to_all | solution.py:118
  152.9 80.3 %all-reduce.5.cloned.1.call-start = ((), (), s32[]{:S(2)}) async-start(), calls=%async_computation.8 | async-start | bytes 786432 | tf_op jit(solution)/shard_map/psum | solution.py:93
  201.5 58.9 %reduce-scatter.8.cloned.1.call-start = ((), (), s32[]{:S(2)}) async-start(), calls=%async_computation.10 | async-start | bytes 1310720 | tf_op jit(solution)/shard_map/reduce_scatter | solution.py:127
  203.7 4.2 %copy-start.7 = (f32[24,2]{0,1:T(2,128)S(1)}, f32[24,2]{0,1:T(2,128)}, u32[]{:S(2)}) copy-start(f32[24,2]{0,1:T(2,128)} %param.36) | copy-start | bytes 580
  203.7 4.2 %copy-start.9 = (f32[24]{0:T(128)S(1)}, f32[24]{0:T(128)}, u32[]{:S(2)}) copy-start(f32[24]{0:T(128)} %param.35) | copy-start | bytes 292
  207.6 58.5 %copy-start.6 = (f32[1024]{0:T(1024)S(1)}, f32[1024]{0:T(1024)}, u32[]{:S(2)}) copy-start(f32[1024]{0:T(1024)} %param.43) | copy-start | bytes 12292
  207.6 118.1 %reduce-scatter.6.cloned.1.call-start = ((), (), s32[]{:S(2)}) async-start(), calls=%async_computation.9 | async-start | bytes 442368 | tf_op jit(solution)/shard_map/reduce_scatter | solution.py:97
  260.4 14.8 %all-to-all-start.2 = ((bf16[8,12,1024]{2,1,0:T(8,128)(2,1)}), bf16[8,12,1024]{2,1,0:T(8,128)(2,1)S(1)}, u32[]{:S(2)}, u32[]{:S(2)}) async-start(bf16[8,12,1024]{2,1,0:T(8,128)(2,1)} %reduce-scatter.8.cloned.1.call-done), calls=%async_computation.5 | async-start | bytes 524288 | tf_op jit(solution)/shard_map/all_to_all | solution.py:130
Sparse Core Ops, SparseCore 0:
  27.4 61.3 reduce-scatter.3
  111.4 31.0 all-reduce.2
  201.7 31.4 all-reduce.4
  235.6 24.7 reduce-scatter.7
  263.5 62.1 reduce-scatter.5
where the time goes:
time: 335 us; the launch traced here: 334 us
  waiting for transfers between devices  197 us (59%)
  blocking collectives  60.7 us (18%)
  matrix products  33.2 us (10%)
  between operations  14.1 us (4%)
  other arithmetic  13.2 us (4%)
  starting transfers between devices  11.2 us (3%)
  local copies, waits for them, and re-layouts  4.25 us (1%)
    reduce_scatter x1, waiting for transfers between devices, per_device(): lax.psum_scatter(jnp.dot(spread, joined, preferred_element_type=jnp.float...  58.6 us
    reduce_scatter x1, waiting for transfers between devices, per_device(): lax.psum_scatter(jnp.dot(dense_hidden, dense_down, preferred_element_type...  49.3 us
    all_gather x1, blocking collectives, per_device(): lax.all_gather(own_columns, 'ep', axis=0, tiled=True)  45.7 us
    psum x1, waiting for transfers between devices, per_device(): lax.psum(attn_part.astype(jnp.bfloat16), 'tp').astype(jnp.float32)  31.2 us
    psum x1, waiting for transfers between devices, per_device(): lax.psum(dense_part.astype(jnp.bfloat16), 'tp').astype(jnp.float32)  25.3 us
    reduce_scatter x1, waiting for transfers between devices, per_device(): lax.psum_scatter(partial_value.astype(jnp.bfloat16), 'tp', scatter_dimens...  23.5 us
    all_to_all x1, blocking collectives, per_device(): lax.all_to_all(normed, 'ep', split_axis=1, concat_axis=0, tiled=True)  15 us
    all_to_all x1, waiting for transfers between devices, per_device(): lax.all_to_all(summed_cols, 'ep', split_axis=0, concat_axis=0, tiled=True)  9.06 us
  transfers between devices with their start and end apart: 7, of which 6 were waited for; matrix products, arithmetic and copies ran while one was open for 5% of the time, Pallas kernels for 0%

commit v1 on v0

--- a/solution.py
+++ b/solution.py
@@ -90,7 +90,9 @@
         gate_up,
         preferred_element_type=jnp.float32,
     )
-    dense_sum = lax.psum(dense_part.astype(jnp.bfloat16), "tp").astype(jnp.float32)
+    dense_sum = jnp.sum(lax.all_gather(dense_part.astype(jnp.bfloat16), "tp"), axis=0).astype(
+        jnp.float32
+    )
     dense_hidden = (jax.nn.silu(dense_sum[:, :hidden_width]) * dense_sum[:, hidden_width:]).astype(
         jnp.bfloat16
     )

time: 335 us -> 309 us (0.922)
  waiting for transfers between devices: 197 us -> 167 us
  blocking collectives: 60.7 us -> 70.3 us
  starting transfers between devices: 11.2 us -> 5.71 us
    psum x1 -> x0, waiting for transfers between devices: 25.3 us -> none  [per_device(): lax.psum(dense_part.astype(jnp.bfloat16), 'tp').astype(jnp.float32)]
    all_to_all x0 -> x1, blocking collectives: none -> 24.1 us  [per_device(): lax.all_to_all(outgoing, 'ep', split_axis=0, concat_axis=0, tiled=True)]
    all_gather x1, blocking collectives: 45.7 us -> 31.2 us  [per_device(): lax.all_gather(own_columns, 'ep', axis=0, tiled=True)]
    all_to_all x1 -> x0, starting transfers between devices: 5.51 us -> none  [per_device(): lax.all_to_all(outgoing, 'ep', split_axis=0, concat_axis=0, tiled=True)]
    reduce_scatter x1, waiting for transfers between devices: 23.5 us -> 18.8 us  [per_device(): lax.psum_scatter(partial_value.astype(jnp.bfloat16), 'tp', scatter_dimens...]
  transfers between devices with their start and end apart: 7 -> 6, of which waited for: 6 -> 5; matrix products, arithmetic and copies ran while one was open for 5% -> 5% of each run, Pallas kernels for 0% -> 0%
where the time goes in v1:
time: 309 us
  waiting for transfers between devices  167 us (54%)
  blocking collectives  70.3 us (23%)
  matrix products  33.2 us (11%)
  between operations  14.2 us (5%)
  other arithmetic  13.9 us (4%)
  starting transfers between devices  5.71 us (2%)
  local copies, waits for them, and re-layouts  4.23 us (1%)
    reduce_scatter x1, waiting for transfers between devices, per_device(): lax.psum_scatter(jnp.dot(spread, joined, preferred_element_type=jnp.float...  58.8 us
    reduce_scatter x1, waiting for transfers between devices, per_device(): lax.psum_scatter(jnp.dot(dense_hidden, dense_down, preferred_element_type...  49.4 us
    all_gather x1, blocking collectives, per_device(): lax.all_gather(own_columns, 'ep', axis=0, tiled=True)  31.2 us
    psum x1, waiting for transfers between devices, per_device(): lax.psum(attn_part.astype(jnp.bfloat16), 'tp').astype(jnp.float32)  31 us
    all_to_all x1, blocking collectives, per_device(): lax.all_to_all(outgoing, 'ep', split_axis=0, concat_axis=0, tiled=True)  24.1 us
    reduce_scatter x1, waiting for transfers between devices, per_device(): lax.psum_scatter(partial_value.astype(jnp.bfloat16), 'tp', scatter_dimens...  18.8 us
    all_to_all x1, blocking collectives, per_device(): lax.all_to_all(normed, 'ep', split_axis=1, concat_axis=0, tiled=True)  15 us
    all_to_all x1, waiting for transfers between devices, per_device(): lax.all_to_all(summed_cols, 'ep', split_axis=0, concat_axis=0, tiled=True)  9 us
  transfers between devices with their start and end apart: 6, of which 5 were waited for; matrix products, arithmetic and copies ran while one was open for 5% of the time, Pallas kernels for 0%

profile of v1, /device:TPU:0, one launch (start us, length us, event | category | flops | bytes accessed | tf_op | source)
XLA Modules:
  0.0 308.6 jit_solution(11541364711296302137)
XLA Ops:
  7.2 1.2 fusion.28
  8.4 1.1 fusion.30
  9.6 15.0 %all_to_all.29 = bf16[24,8,512]{2,0,1:T(8,128)(2,1)S(1)} all-to-all(bf16[24,8,512]{2,0,1:T(8,128)(2,1)S(1)} %bitcast.61), channel_id=1, replica_groups=mesh['ep'=8,'tp'=4] {'ep'}, dimensions={1} | all-to-all | bytes 393216 | tf_op jit(solution)/shard_map/all_to_all | solution.py:49
  24.6 2.7 convolution_convert_fusion.3
  30.0 58.8 %reduce-scatter.4.cloned.1.call-done = bf16[24,1536]{1,0:T(8,128)(2,1)} async-done(((bf16[192,1536]{1,0:T(8,128)(2,1)}), bf16[24,1536]{1,0:T(8,128)(2,1)}) %reduce-scatter.4.cloned.1.call-update) | async-done | bytes 73744 | tf_op jit(solution)/shard_map/reduce_scatter | solution.py:51
  89.8 8.1 %fusion.59 = f32[24,4,1,128]{3,2,1,0:T(1,128)S(1)} fusion(f32[24,4,128,1]{2,3,1,0:T(1,128)S(1)} %bitcast.62, f32[24,4,128,128]{3,2,1,0:T(8,128)} %param.23), kind=kOutput, calls=%fused_computation.93 | convolution fusion | flops 18874368 | bytes 6389760 | tf_op jit(solution)/shard_map/bhk,bhkv->bhv/dot_general | solution.py:73
  98.1 3.9 %multiply_add_fusion = f32[24,4,128,128]{3,2,1,0:T(8,128)} fusion(f32[24,4,128,128]{3,2,1,0:T(8,128)S(1)} %copy-done.1, f32[24,4,128]{2,1,0:T(4,128)S(1)} %subtract_multiply_fusion, f32[24,4,128]{2,1,0:T(4,128)S(1)} %broadcast_multiply_fusion, f32[24,4]{1,0:T(8,128)S(1)} %copy.67), kind=kLoop, calls=%fused_computation.1 | loop fusion | flops 4718592 | bytes 12681600 | tf_op jit(solution)/shard_map/add | solution.py:76
  102.2 7.5 %fusion.60 = f32[24,4,1,128]{3,2,1,0:T(1,128)S(1)} fusion(f32[24,4,128,1]{2,3,1,0:T(1,128)S(1)} %bitcast.65, f32[24,4,128,128]{3,2,1,0:T(8,128)} %multiply_add_fusion), kind=kOutput, calls=%fused_computation.94 | convolution fusion | flops 18874368 | bytes 6389760 | tf_op jit(solution)/shard_map/bhk,bhkv->bhv/dot_general | solution.py:78
  109.9 1.4 convolution_convert_fusion.2
  111.5 31.0 %all-reduce.2.cloned.1.call-done = bf16[24,4096]{1,0:T(8,128)(2,1)} async-done(((bf16[24,4096]{1,0:T(8,128)(2,1)}), bf16[24,4096]{1,0:T(8,128)(2,1)}) %all-reduce.2.cloned.1.call-update) | async-done | bytes 196624 | tf_op jit(solution)/shard_map/psum | solution.py:81
  142.5 1.8 convert_add_fusion
  145.4 31.2 %all_gather.9 = bf16[192,1024]{1,0:T(8,128)(2,1)S(1)} all-gather(bf16[24,1024]{1,0:T(8,128)(2,1)S(1)} %constant_dynamic-slice_fusion), channel_id=1, replica_groups=mesh['ep'=8,'tp'=4] {'ep'}, dimensions={0}, use_global_device_ids=true | all-gather | bytes 442368 | tf_op jit(solution)/shard_map/all_gather | solution.py:89
  176.6 2.9 fusion.14
  180.4 1.1 reshape.153
  181.6 24.1 %all_to_all.30 = bf16[8,12,4096]{2,1,0:T(8,128)(2,1)S(1)} all-to-all(bf16[8,12,4096]{2,1,0:T(8,128)(2,1)} %reshape.153), channel_id=1, replica_groups=mesh['ep'=8,'tp'=4] {'ep'}, dimensions={0} | all-to-all | bytes 1572864 | tf_op jit(solution)/shard_map/all_to_all | solution.py:120
  205.6 2.0 fusion.7
  207.7 3.9 %convolution_convert_fusion = bf16[8,12,4096]{2,1,0:T(8,128)(2,1)} fusion(bf16[1,256,4096]{2,1,0:T(8,128)(2,1)S(1)} %copy-done, bf16[8,12,4096]{2,1,0:T(8,128)(2,1)S(1)} %all_to_all.30, bf16[1,4096,256]{2,1,0:T(8,128)(2,1)} %param.38, f32[8,12,256]{2,1,0:T(8,128)S(1)} %fusion.7), kind=kOutput, calls=%fused_computation.2 | convolution fusion | flops 403193856 | bytes 5865472 | tf_op jit(solution)/shard_map/snf,fd->snd/dot_general | solution.py:126
  212.0 1.7 reduce_sum.93
  213.8 2.4 convolution_convert_fusion.4
  216.4 18.8 %reduce-scatter.8.cloned.1.call-done = bf16[8,12,1024]{2,1,0:T(8,128)(2,1)} async-done(((bf16[8,12,4096]{2,1,0:T(8,128)(2,1)}), bf16[8,12,1024]{2,1,0:T(8,128)(2,1)}) %reduce-scatter.8.cloned.1.call-update) | async-done | bytes 196624 | tf_op jit(solution)/shard_map/reduce_scatter | solution.py:129
  235.2 5.5 %all-to-all-start.2 = ((bf16[8,12,1024]{2,1,0:T(8,128)(2,1)}), bf16[8,12,1024]{2,1,0:T(8,128)(2,1)S(1)}, u32[]{:S(2)}, u32[]{:S(2)}) async-start(bf16[8,12,1024]{2,1,0:T(8,128)(2,1)} %reduce-scatter.8.cloned.1.call-done), calls=%async_computation.5 | async-start | bytes 524288 | tf_op jit(solution)/shard_map/all_to_all | solution.py:132
  240.9 9.0 %all-to-all-done.2 = bf16[8,12,1024]{2,1,0:T(8,128)(2,1)S(1)} async-done(((bf16[8,12,1024]{2,1,0:T(8,128)(2,1)}), bf16[8,12,1024]{2,1,0:T(8,128)(2,1)S(1)}, u32[]{:S(2)}, u32[]{:S(2)}) %all-to-all-start.2) | async-done | bytes 196640 | tf_op jit(solution)/shard_map/all_to_all | solution.py:132
  251.1 49.4 %reduce-scatter.6.cloned.1.call-done = bf16[24,1024]{1,0:T(8,128)(2,1)} async-done(((bf16[192,1024]{1,0:T(8,128)(2,1)}), bf16[24,1024]{1,0:T(8,128)(2,1)}) %reduce-scatter.6.cloned.1.call-update) | async-done | bytes 49168 | tf_op jit(solution)/shard_map/reduce_scatter | solution.py:99
  300.5 1.6 add_convert_fusion
  (84 shorter events, 8.4 us)
Async XLA Ops:
  7.2 200.5 %copy-start = (bf16[1,256,4096]{2,1,0:T(8,128)(2,1)S(1)}, bf16[1,256,4096]{2,1,0:T(8,128)(2,1)}, u32[]{:S(2)}) copy-start(bf16[1,256,4096]{2,1,0:T(8,128)(2,1)} %param.39) | copy-start | bytes 6291460
  7.2 81.6 %reduce-scatter.4.cloned.1.call-start = ((), (), s32[]{:S(2)}) async-start(), calls=%async_computation.6 | async-start | bytes 663552 | tf_op jit(solution)/shard_map/reduce_scatter | solution.py:51
  9.5 17.8 %copy-start.10 = (f32[4]{0:T(128)S(1)}, f32[4]{0:T(128)}, u32[]{:S(2)}) copy-start(f32[4]{0:T(128)} %param.30) | copy-start | bytes 52
  9.5 20.1 %copy-start.5 = (s32[24,2]{0,1:T(2,128)S(1)}, s32[24,2]{0,1:T(2,128)}, u32[]{:S(2)}) copy-start(s32[24,2]{0,1:T(2,128)} %param.34) | copy-start | bytes 580
  27.3 115.2 %all-reduce.2.cloned.1.call-start = ((), (), s32[]{:S(2)}) async-start(), calls=%async_computation.7 | async-start | bytes 393216 | tf_op jit(solution)/shard_map/psum | solution.py:81
  89.8 8.2 %copy-start.1 = (f32[24,4,128,128]{3,2,1,0:T(8,128)S(1)}, f32[24,4,128,128]{3,2,1,0:T(8,128)}, u32[]{:S(2)}) copy-start(f32[24,4,128,128]{3,2,1,0:T(8,128)} %param.23) | copy-start | bytes 18874372
  102.2 7.6 %copy-start.8 = (f32[128]{0:T(128)S(1)}, f32[128]{0:T(128)}, u32[]{:S(2)}) copy-start(f32[128]{0:T(128)} %param.31) | copy-start | bytes 1540
  102.2 7.7 %copy-start.2 = (bf16[512,4096]{1,0:T(8,128)(2,1)S(1)}, bf16[512,4096]{1,0:T(8,128)(2,1)}, u32[]{:S(2)}) copy-start(bf16[512,4096]{1,0:T(8,128)(2,1)} %param.32) | copy-start | bytes 12582916
  109.7 32.8 %copy-start.3 = (bf16[24,4096]{1,0:T(8,128)(2,1)S(1)}, bf16[24,4096]{1,0:T(8,128)(2,1)}, u32[]{:S(2)}) copy-start(bf16[24,4096]{1,0:T(8,128)(2,1)} %param.22) | copy-start | bytes 589828
  109.7 34.7 %copy-start.4 = (f32[4096]{0:T(1024)S(1)}, f32[4096]{0:T(1024)}, u32[]{:S(2)}) copy-start(f32[4096]{0:T(1024)} %param.33) | copy-start | bytes 49156
  111.3 100.7 %all-gather.3.cloned.1.call-start = ((), (), s32[]{:S(2)}) async-start(), calls=%async_computation.10 | async-start | bytes 1966080 | tf_op jit(solution)/shard_map/all_gather | solution.py:93
  179.5 55.7 %reduce-scatter.8.cloned.1.call-start = ((), (), s32[]{:S(2)}) async-start(), calls=%async_computation.9 | async-start | bytes 1310720 | tf_op jit(solution)/shard_map/reduce_scatter | solution.py:129
  207.7 4.2 %copy-start.7 = (f32[24,2]{0,1:T(2,128)S(1)}, f32[24,2]{0,1:T(2,128)}, u32[]{:S(2)}) copy-start(f32[24,2]{0,1:T(2,128)} %param.36) | copy-start | bytes 580
  207.7 4.2 %copy-start.9 = (f32[24]{0:T(128)S(1)}, f32[24]{0:T(128)}, u32[]{:S(2)}) copy-start(f32[24]{0:T(128)} %param.35) | copy-start | bytes 292
  211.6 88.8 %reduce-scatter.6.cloned.1.call-start = ((), (), s32[]{:S(2)}) async-start(), calls=%async_computation.8 | async-start | bytes 442368 | tf_op jit(solution)/shard_map/reduce_scatter | solution.py:99
  211.9 29.0 %copy-start.6 = (f32[1024]{0:T(1024)S(1)}, f32[1024]{0:T(1024)}, u32[]{:S(2)}) copy-start(f32[1024]{0:T(1024)} %param.43) | copy-start | bytes 12292
  235.2 14.7 %all-to-all-start.2 = ((bf16[8,12,1024]{2,1,0:T(8,128)(2,1)}), bf16[8,12,1024]{2,1,0:T(8,128)(2,1)S(1)}, u32[]{:S(2)}, u32[]{:S(2)}) async-start(bf16[8,12,1024]{2,1,0:T(8,128)(2,1)} %reduce-scatter.8.cloned.1.call-done), calls=%async_computation.5 | async-start | bytes 524288 | tf_op jit(solution)/shard_map/all_to_all | solution.py:132
Sparse Core Ops, SparseCore 0:
  27.4 61.3 reduce-scatter.3
  111.4 31.0 all-reduce.1
  179.7 19.3 all-gather.2
  211.7 23.4 reduce-scatter.7
  238.3 62.1 reduce-scatter.5
